TPU v7x, 256 devices: a 2x2x32 block of a 4x8x32 slice. The times are simulated.
256 devices in a mesh: grp: 4 (over y, x), ep: 64 (over z, core).
Axes of the slice: x: 2, y: 2, z: 32, core: 2. Of those that a mesh axis runs over, the one named last changes fastest.
The devices are a block of a 4x8x32 slice.
Arguments:
- tokens: bfloat16 [8192, 2048], P(('grp', 'ep')), parts along dimension 0, may hold values from -6 to 6
- norm_gain: float32 [2048], replicated, may hold values from 0.1 to 1.9
- routing: int32 [8192, 8], P(('grp', 'ep')), parts along dimension 0, may hold values from 0 to 63, all different within a row; in each aligned block of 32 rows (0 to 31, 32 to 63, ...) at most 8 rows name the same one
- gates: float32 [8192, 8], P(('grp', 'ep')), parts along dimension 0, may hold values from 0.05 to 0.6
- w_gate: bfloat16 [64, 2048, 512], P('ep'), may hold values from -0.125 to 0.125
- w_up: bfloat16 [64, 2048, 512], P('ep'), may hold values from -0.125 to 0.125
- w_down: bfloat16 [64, 512, 2048], P('ep'), may hold values from -0.25 to 0.25
- shared_gate: bfloat16 [2048, 512], replicated, may hold values from -0.125 to 0.125
- shared_up: bfloat16 [2048, 512], replicated, may hold values from -0.125 to 0.125
- shared_down: bfloat16 [512, 2048], replicated, may hold values from -0.25 to 0.25
Outputs:
- mixed: bfloat16 [8192, 2048], P(('grp', 'ep')), parts along dimension 0
There are 4 independent parts, one for each index of `grp`. A program takes and returns all parts, laid end to end along the dimension named above; an argument that names none is the same for every part. Nothing has to cross between parts.
Inputs may be any that keep to these rules, and one draw needn't show every extreme that they name: `routing`: within the 32 rows of one device no expert is named by more than 8 rows, and in every draw some expert is named by exactly 8 rows of some device; each row names 8 different experts.
All inputs are finite; a program needn't handle non-finite values.
Results may differ from a plain program's by a relative error of at most 0.0067.
Values may be sent and summed in bfloat16 or wider, within the bound.
A program may use at most 128 MiB of HBM per device.

v0:
```python
import jax
import jax.numpy as jnp
from jax import lax
from jax.sharding import PartitionSpec as P

epsilon = 1e-06


def rms_normed(tokens, norm_gain):
    floats = tokens.astype(jnp.float32)
    scale_inv = lax.rsqrt(jnp.mean(floats * floats, axis=-1, keepdims=True) + epsilon)
    return (floats * scale_inv * norm_gain).astype(jnp.bfloat16)


def body(
    tokens, norm_gain, routing, gates, w_gate, w_up, w_down, shared_gate, shared_up, shared_down
):
    normed = rms_normed(tokens, norm_gain)
    shared_hidden = (
        jax.nn.silu(jnp.dot(normed, shared_gate, preferred_element_type=jnp.float32))
        * jnp.dot(normed, shared_up, preferred_element_type=jnp.float32)
    ).astype(jnp.bfloat16)
    shared_out = jnp.dot(shared_hidden, shared_down, preferred_element_type=jnp.float32)
    everyone = lax.all_gather(normed, "ep", axis=0, tiled=True)
    routes = lax.all_gather(routing, "ep", axis=0, tiled=True)
    weights = lax.all_gather(gates, "ep", axis=0, tiled=True)
    own = lax.axis_index("ep")
    scale = jnp.sum(jnp.where(routes == own, weights, 0.0), axis=-1, keepdims=True)
    hidden = (
        jax.nn.silu(jnp.dot(everyone, w_gate[0], preferred_element_type=jnp.float32))
        * jnp.dot(everyone, w_up[0], preferred_element_type=jnp.float32)
        * scale
    )
    part = jnp.dot(
        hidden.astype(jnp.bfloat16), w_down[0], preferred_element_type=jnp.float32
    ).astype(jnp.bfloat16)
    routed = lax.psum_scatter(part, "ep", scatter_dimension=0, tiled=True)
    return (shared_out + routed.astype(jnp.float32)).astype(jnp.bfloat16)


def solution(mesh):
    placed = (
        P(("grp", "ep"), None),
        P(),
        P(("grp", "ep"), None),
        P(("grp", "ep"), None),
        P("ep", None, None),
        P("ep", None, None),
        P("ep", None, None),
        P(),
        P(),
        P(),
    )
    return jax.shard_map(
        body, mesh=mesh, in_specs=placed, out_specs=P(("grp", "ep"), None), check_vma=False
    )
```

profile of v0, /device:TPU:38, one launch (start us, length us, event | category | flops | bytes accessed | tf_op | source)
XLA Modules:
  0.0 402.0 jit_solution(2111920116285077826)
XLA Ops:
  6.5 0.0 copy-start
  6.6 0.0 all-gather.4.cloned.1.call-start
  6.6 1.2 fusion.6
  7.7 1.7 fusion.8
  9.4 0.1 all-gather.4.cloned.1.call-update
  9.5 0.1 reduce-scatter.2.cloned.1.call-start
  9.6 76.1 %all-gather = s32[64,32,8]{1,2,0:T(8,128)S(1)} all-gather(s32[1,32,8]{1,2,0:T(8,128)} %bitcast.19), channel_id=1, replica_groups=mesh['grp'=4,'ep'=64] {'ep'}, dimensions={0}, use_global_device_ids=true | all-gather | bytes 66560 | tf_op jit(solution)/shard_map/all_gather | solution.py:25
  85.6 53.4 %all-gather.1 = f32[64,32,8]{1,2,0:T(8,128)S(1)} all-gather(f32[1,32,8]{1,2,0:T(8,128)} %bitcast.20), channel_id=1, replica_groups=mesh['grp'=4,'ep'=64] {'ep'}, dimensions={0}, use_global_device_ids=true | all-gather | bytes 66560 | tf_op jit(solution)/shard_map/all_gather | solution.py:26
  139.0 0.1 select_reduce_fusion
  139.1 0.1 reshape.18
  139.2 20.5 %all-gather.4.cloned.1.call-done = bf16[2048,2048]{1,0:T(8,128)(2,1)} async-done(((bf16[32,2048]{1,0:T(8,128)(2,1)}), bf16[2048,2048]{1,0:T(8,128)(2,1)}) %all-gather.4.cloned.1.call-update) | async-done | bytes 8388624 | tf_op jit(solution)/shard_map/all_gather | solution.py:24
  159.7 0.0 copy-start.2
  159.7 0.0 copy-start.3
  159.7 7.7 %fusion.3 = f32[2048,512]{1,0:T(8,128)S(1)} fusion(bf16[2048,2048]{1,0:T(8,128)(2,1)} %all-gather.4.cloned.1.call-done, bf16[1,2048,512]{2,1,0:T(8,128)(2,1)} %param.14), kind=kOutput, calls=%fused_computation.6 | convolution fusion | flops 4294967296 | bytes 14680064 | tf_op jit(solution)/shard_map/dot_general | solution.py:30
  167.4 0.0 copy-done.2
  167.4 0.0 copy-done.3
  167.4 5.2 %multiply_convert_fusion = bf16[2048,512]{1,0:T(8,128)(2,1)S(1)} fusion(f32[2048,512]{1,0:T(8,128)S(1)} %fusion.3, bf16[2048,2048]{1,0:T(8,128)(2,1)S(1)} %copy-done.2, bf16[1,2048,512]{2,1,0:T(8,128)(2,1)S(1)} %copy-done.3, f32[2048]{0:T(1024)S(1)} %reshape.18), kind=kOutput, calls=%fused_computation.1 | convolution fusion | flops 4302307328 | bytes 16785408 | tf_op jit(solution)/shard_map/dot_general | solution.py:31
  172.7 0.0 copy-done
  172.7 6.8 %convolution_convert_fusion = bf16[2048,2048]{1,0:T(8,128)(2,1)} fusion(bf16[2048,512]{1,0:T(8,128)(2,1)S(1)} %multiply_convert_fusion, bf16[1,512,2048]{2,1,0:T(8,128)(2,1)S(1)} %copy-done), kind=kOutput, calls=%fused_computation | convolution fusion | flops 4299161600 | bytes 12582912 | tf_op jit(solution)/shard_map/dot_general | solution.py:34
  179.5 0.0 copy-start.1
  179.5 0.1 reduce-scatter.2.cloned.1.call-update
  179.5 0.8 copy-done.1
  180.4 2.0 fusion.16
  182.4 209.0 %reduce-scatter.2.cloned.1.call-done = bf16[32,2048]{1,0:T(8,128)(2,1)} async-done(((bf16[2048,2048]{1,0:T(8,128)(2,1)}), bf16[32,2048]{1,0:T(8,128)(2,1)}) %reduce-scatter.2.cloned.1.call-update) | async-done | bytes 131088 | tf_op jit(solution)/shard_map/reduce_scatter | solution.py:37
  391.4 3.8 fusion
  (1 shorter events, 0.0 us)
Async XLA Ops:
  6.5 166.1 %copy-start = (bf16[1,512,2048]{2,1,0:T(8,128)(2,1)S(1)}, bf16[1,512,2048]{2,1,0:T(8,128)(2,1)}, u32[]{:S(2)}) copy-start(bf16[1,512,2048]{2,1,0:T(8,128)(2,1)} %param.16) | copy-start | bytes 6291460
  6.6 153.2 %all-gather.4.cloned.1.call-start = ((), (), s32[]{:S(2)}) async-start(), calls=%async_computation.1 | async-start | bytes 8519680 | tf_op jit(solution)/shard_map/all_gather | solution.py:24
  9.5 381.9 %reduce-scatter.2.cloned.1.call-start = ((), (), s32[]{:S(2)}) async-start(), calls=%async_computation.2 | async-start | bytes 8519680 | tf_op jit(solution)/shard_map/reduce_scatter | solution.py:37
  159.7 7.7 %copy-start.2 = (bf16[2048,2048]{1,0:T(8,128)(2,1)S(1)}, bf16[2048,2048]{1,0:T(8,128)(2,1)}, u32[]{:S(2)}) copy-start(bf16[2048,2048]{1,0:T(8,128)(2,1)} %all-gather.4.cloned.1.call-done) | copy-start | bytes 25165828
  159.7 7.7 %copy-start.3 = (bf16[1,2048,512]{2,1,0:T(8,128)(2,1)S(1)}, bf16[1,2048,512]{2,1,0:T(8,128)(2,1)}, u32[]{:S(2)}) copy-start(bf16[1,2048,512]{2,1,0:T(8,128)(2,1)} %param.15) | copy-start | bytes 6291460
  179.5 0.9 copy-start.1
Sparse Core Ops, SparseCore 0:
  9.6 150.0 all-gather.3
  179.6 211.6 reduce-scatter.1
where the time goes:
time: 402 us
  waiting for transfers between devices  230 us (57%)
  blocking collectives  129 us (32%)
  matrix products  25.5 us (6%)
  between operations  13.5 us (3%)
    reduce_scatter x1, waiting for transfers between devices, body(): routed = lax.psum_scatter(part, 'ep', scatter_dimension=0, tiled=True)  209 us
    all_gather x1, blocking collectives, body(): routes = lax.all_gather(routing, 'ep', axis=0, tiled=True)  76.1 us
    all_gather x1, blocking collectives, body(): weights = lax.all_gather(gates, 'ep', axis=0, tiled=True)  53.4 us
    all_gather x1, waiting for transfers between devices, body(): everyone = lax.all_gather(normed, 'ep', axis=0, tiled=True)  20.5 us
  transfers between devices with their start and end apart: 2, of which 2 were waited for; matrix products, arithmetic and copies ran while one was open for 1% of the time, Pallas kernels for 0%

commit v1 on v0

--- a/solution.py
+++ b/solution.py
@@ -21,7 +21,11 @@
         * jnp.dot(normed, shared_up, preferred_element_type=jnp.float32)
     ).astype(jnp.bfloat16)
     shared_out = jnp.dot(shared_hidden, shared_down, preferred_element_type=jnp.float32)
-    everyone = lax.all_gather(normed, "ep", axis=0, tiled=True)
+    size = lax.axis_size("ep")
+    repeats = [size if d == 0 else 1 for d in range(normed.ndim)]
+    everyone = lax.all_to_all(
+        jnp.tile(normed, repeats), "ep", split_axis=0, concat_axis=0, tiled=True
+    )
     routes = lax.all_gather(routing, "ep", axis=0, tiled=True)
     weights = lax.all_gather(gates, "ep", axis=0, tiled=True)
     own = lax.axis_index("ep")

time: 402 us -> 1130 us (2.81)
  blocking collectives: 129 us -> 827 us
  starting transfers between devices: 0.07 us -> 34.5 us
  waiting for transfers between devices: 230 us -> 214 us
    all_gather x1, blocking collectives: 76.1 us -> 771 us  [body(): routes = lax.all_gather(routing, 'ep', axis=0, tiled=True)]
    all_to_all x0 -> x1, starting transfers between devices: none -> 34.4 us  [body(): lax.all_to_all(jnp.tile(normed, repeats), 'ep', split_axis=0, concat_axis...]
    all_gather x1 -> x0, waiting for transfers between devices: 20.5 us -> none  [body(): everyone = lax.all_gather(normed, 'ep', axis=0, tiled=True)]
  transfers between devices with their start and end apart: 2 -> 2, of which waited for: 2 -> 1; matrix products, arithmetic and copies ran while one was open for 1% -> 0% of each run, Pallas kernels for 0% -> 0%
where the time goes in v1:
time: 1130 us; the launch traced here: 1120 us
  blocking collectives  827 us (73%)
  waiting for transfers between devices  214 us (19%)
  starting transfers between devices  34.5 us (3%)
  matrix products  29.1 us (3%)
  between operations  13.5 us (1%)
    all_gather x1, blocking collectives, body(): routes = lax.all_gather(routing, 'ep', axis=0, tiled=True)  771 us
    reduce_scatter x1, waiting for transfers between devices, body(): routed = lax.psum_scatter(part, 'ep', scatter_dimension=0, tiled=True)  214 us
    all_gather x1, blocking collectives, body(): weights = lax.all_gather(gates, 'ep', axis=0, tiled=True)  55.5 us
    all_to_all x1, starting transfers between devices, body(): lax.all_to_all(jnp.tile(normed, repeats), 'ep', split_axis=0, concat_axis...  34.4 us
  transfers between devices with their start and end apart: 2, of which 1 were waited for; matrix products, arithmetic and copies ran while one was open for 0% of the time, Pallas kernels for 0%

profile of v1, /device:TPU:38, one launch (start us, length us, event | category | flops | bytes accessed | tf_op | source)
XLA Modules:
  0.0 1125.0 jit_solution(9212282284365409099)
XLA Ops:
  6.5 0.0 copy-start
  6.6 1.2 fusion.6
  7.7 1.0 fusion.8
  8.8 4.3 tile.2
  13.0 0.0 copy-start.1
  13.0 0.0 copy-start.2
  13.0 34.4 %all-to-all-start = ((bf16[64,32,2048]{2,1,0:T(8,128)(2,1)}), bf16[64,32,2048]{2,1,0:T(8,128)(2,1)}, u32[]{:S(2)}, u32[]{:S(2)}) async-start(bf16[64,32,2048]{2,1,0:T(8,128)(2,1)} %tile.2), calls=%async_computation | async-start | bytes 16777216 | tf_op jit(solution)/shard_map/all_to_all | solution.py:26
  47.4 0.1 reduce-scatter.2.cloned.1.call-start
  47.5 0.0 copy-done.1
  47.5 771.4 %all-gather = s32[64,32,8]{1,2,0:T(8,128)S(1)} all-gather(s32[1,32,8]{1,2,0:T(8,128)S(1)} %bitcast.20), channel_id=1, replica_groups=mesh['grp'=4,'ep'=64] {'ep'}, dimensions={0}, use_global_device_ids=true | all-gather | bytes 66560 | tf_op jit(solution)/shard_map/all_gather | solution.py:29
  819.0 0.0 copy-done.2
  819.0 55.5 %all-gather.1 = f32[64,32,8]{1,2,0:T(8,128)S(1)} all-gather(f32[1,32,8]{1,2,0:T(8,128)S(1)} %bitcast.21), channel_id=1, replica_groups=mesh['grp'=4,'ep'=64] {'ep'}, dimensions={0}, use_global_device_ids=true | all-gather | bytes 66560 | tf_op jit(solution)/shard_map/all_gather | solution.py:30
  874.4 0.1 select_reduce_fusion
  874.5 0.1 reshape.25
  874.6 0.0 all-to-all-done
  874.6 0.0 copy-start.3
  874.6 7.7 fusion.3
  882.3 0.0 copy-done.3
  882.3 8.9 multiply_convert_fusion
  891.2 0.0 copy-done
  891.2 6.7 convolution_convert_fusion
  898.0 0.1 reduce-scatter.2.cloned.1.call-update
  898.0 2.0 fusion.16
  900.1 214.3 %reduce-scatter.2.cloned.1.call-done = bf16[32,2048]{1,0:T(8,128)(2,1)} async-done(((bf16[2048,2048]{1,0:T(8,128)(2,1)}), bf16[32,2048]{1,0:T(8,128)(2,1)}) %reduce-scatter.2.cloned.1.call-update) | async-done | bytes 131088 | tf_op jit(solution)/shard_map/reduce_scatter | solution.py:41
  1114.3 3.8 fusion
  (1 shorter events, 0.0 us)
Async XLA Ops:
  6.5 884.7 %copy-start = (bf16[1,512,2048]{2,1,0:T(8,128)(2,1)S(1)}, bf16[1,512,2048]{2,1,0:T(8,128)(2,1)}, u32[]{:S(2)}) copy-start(bf16[1,512,2048]{2,1,0:T(8,128)(2,1)} %param.16) | copy-start | bytes 6291460
  13.0 34.5 %copy-start.1 = (s32[32,8]{0,1:T(8,128)S(1)}, s32[32,8]{0,1:T(8,128)}, u32[]{:S(2)}) copy-start(s32[32,8]{0,1:T(8,128)} %param.12) | copy-start | bytes 3076
  13.0 805.9 %copy-start.2 = (f32[32,8]{0,1:T(8,128)S(1)}, f32[32,8]{0,1:T(8,128)}, u32[]{:S(2)}) copy-start(f32[32,8]{0,1:T(8,128)} %param.13) | copy-start | bytes 3076
  13.0 861.6 %all-to-all-start = ((bf16[64,32,2048]{2,1,0:T(8,128)(2,1)}), bf16[64,32,2048]{2,1,0:T(8,128)(2,1)}, u32[]{:S(2)}, u32[]{:S(2)}) async-start(bf16[64,32,2048]{2,1,0:T(8,128)(2,1)} %tile.2), calls=%async_computation | async-start | bytes 16777216 | tf_op jit(solution)/shard_map/all_to_all | solution.py:26
  47.4 1066.9 %reduce-scatter.2.cloned.1.call-start = ((), (), s32[]{:S(2)}) async-start(), calls=%async_computation.2 | async-start | bytes 8519680 | tf_op jit(solution)/shard_map/reduce_scatter | solution.py:41
  874.6 7.7 copy-start.3
Sparse Core Ops, SparseCore 0:
  898.1 216.1 reduce-scatter.1
